TPU v7x, 128 devices: a whole 4x4x4 slice. The times are simulated.
128 devices in a mesh: sp: 16 (over z, y), tp: 8 (over x, core).
Axes of the slice: x: 4, y: 4, z: 4, core: 2. Of those that a mesh axis runs over, the one named last changes fastest.
Arguments:
- query_proj: bfloat16 [16384, 2048], P('sp', 'tp'), may hold values from -6 to 6
- key_proj: bfloat16 [16384, 2048], P('sp', 'tp'), may hold values from -6 to 6
- value_proj: bfloat16 [16384, 4096], P('sp', 'tp'), may hold values from -6 to 6
- gate_proj: bfloat16 [16384, 4096], P('sp', 'tp'), may hold values from -6 to 6
- log_decay: float32 [16384, 8], P('sp', 'tp'), may hold values from -0.75 to 0, as said below
- residual: bfloat16 [16384, 2048], P('sp'), may hold values from -4 to 4
- out_weight: bfloat16 [4096, 2048], P('tp'), may hold values from -0.09375 to 0.09375
- norm_gain: float32 [2, 2048], replicated, may hold values from 0.1 to 1.9
- norm_bias: float32 [2, 2048], replicated, may hold values from -1.5 to 1.5
- up_gate: bfloat16 [2048, 5632], P('sp', 'tp'), may hold values from -0.125 to 0.125
- up_value: bfloat16 [2048, 5632], P('sp', 'tp'), may hold values from -0.125 to 0.125
- conv_weight: float32 [2, 3, 5632], P(None, None, 'tp'), may hold values from -3 to 3
- conv_bias: float32 [2, 5632], P(None, 'tp'), may hold values from -1.5 to 1.5
- down_weight: bfloat16 [5632, 2048], P('tp', 'sp'), may hold values from -0.078125 to 0.078125
Outputs:
- layer_output: bfloat16 [16384, 2048], P(('sp', 'tp'))
Inputs may be any that keep to these rules, and one draw needn't show every extreme that they name: `log_decay`: all entries are negative.
All inputs are finite; a program needn't handle non-finite values.
Results may differ from a plain program's by a relative error of at most 0.023.
Values may be sent and summed in bfloat16 or wider, within the bound.
No kernel may reach another device: no remote copies, remote signals or barrier semaphores. Data moves between devices by JAX's collectives and lax.ppermute only.
A program may use at most 128 MiB of HBM per device.

v0:
```python
import jax
import jax.numpy as jnp
from jax import lax
from jax.sharding import Mesh
from jax.sharding import PartitionSpec as P

BLOCK = 256
SP = ("sp_0", "sp_1")
SP_TP = ("sp_0", "sp_1", "tp")
alpha_scale = 8.0**0.25
rope_base = 10000.0
tiny_stabilizer = 1e-05


def turned_gather(arrays, axis, dims):
    turned = [jnp.moveaxis(a, dim, 0) for a, dim in zip(arrays, dims)]
    both = jnp.concatenate([t.reshape(len(t), -1) for t in turned], axis=1)
    out, at, finished = (lax.all_gather(both, axis, axis=0, tiled=True), 0, [])
    for t, dim in zip(turned, dims):
        piece = out[:, at : at + t[0].size].reshape(-1, *t.shape[1:])
        finished.append(jnp.moveaxis(piece, 0, dim))
        at += t[0].size
    return tuple(finished)


def neutral_like(x, identity):
    return jax.tree.map(
        lambda a, e: jnp.broadcast_to(jnp.asarray(e, a.dtype), a.shape), x, identity
    )


def entering(x, axes, combine, identity):
    before = start = neutral_like(x, identity)
    subtotal = x
    for axis in reversed(axes):
        length, position = (lax.axis_size(axis), lax.axis_index(axis))
        pieces = jax.tree.map(
            lambda part, kind: lax.all_gather(part.astype(kind), axis),
            subtotal,
            (jnp.bfloat16, jnp.bfloat16),
        )
        inside, subtotal = (start, start)
        for k in range(length):
            passed = k < position
            subtotal = combine(
                subtotal, jax.tree.map(lambda part, own: part[k].astype(own.dtype), pieces, x)
            )
            inside = jax.tree.map(lambda new, old: jnp.where(passed, new, old), subtotal, inside)
        before = combine(inside, before)
    return before


def passed_along(x, axis, by):
    length = lax.axis_size(axis)
    pairs = [(i, i + by) for i in range(length) if 0 <= i + by < length]
    return lax.ppermute(x, axis, pairs)


def rotate(vectors, positions):
    head_width = vectors.shape[-1]
    half_width = head_width // 2
    inverse_freq = rope_base ** (-2.0 * jnp.arange(half_width, dtype=jnp.float32) / head_width)
    angles = positions[:, None] * inverse_freq[None, :]
    cosine = jnp.cos(angles)[:, None, :]
    sine_part = jnp.sin(angles)[:, None, :]
    front = vectors[..., :half_width]
    second = vectors[..., half_width:]
    return jnp.concatenate(
        [front * cosine - second * sine_part, front * sine_part + second * cosine], axis=-1
    )


def layer_norm(values, gain, shift):
    average = values.mean(-1, keepdims=True)
    spread = jnp.square(values - average).mean(-1, keepdims=True)
    return (values - average) * lax.rsqrt(spread + tiny_stabilizer) * gain + shift


def block_parts(query_tile, lookup_piece, payload_piece, log_blk):
    cum_log = jnp.cumsum(log_blk, axis=0)
    cum_heads = cum_log.T
    log_gap = cum_heads[:, :, None] - cum_heads[:, None, :]
    offsets = jnp.arange(log_blk.shape[0])
    causal = (offsets[:, None] >= offsets[None, :])[None]
    weight = jnp.where(causal, jnp.exp(jnp.where(causal, log_gap, 0.0)), 0.0)
    score_matrix = jnp.einsum(
        "jka,ska->kjs", query_tile, lookup_piece, preferred_element_type=jnp.float32
    )
    segment_scaling = (score_matrix * weight).astype(jnp.bfloat16)
    within = jnp.einsum(
        "htm,mhe->the", segment_scaling, payload_piece, preferred_element_type=jnp.float32
    )
    block_total = cum_log[-1]
    to_end = jnp.exp(block_total[None, :] - cum_log)
    faded_lookup_vector = (lookup_piece.astype(jnp.float32) * to_end[:, :, None]).astype(
        jnp.bfloat16
    )
    summand_term = jnp.einsum(
        "ajo,ajd->jod", faded_lookup_vector, payload_piece, preferred_element_type=jnp.float32
    )
    scaled_query = (query_tile.astype(jnp.float32) * jnp.exp(cum_log)[:, :, None]).astype(
        jnp.bfloat16
    )
    return (within, scaled_query, summand_term, jnp.exp(block_total))


def causal_conv(rows, edge_rows, taps, shift):
    padded = jnp.concatenate([edge_rows, rows], axis=0).astype(jnp.float32)
    length = rows.shape[0]
    result = shift[None, :] + padded[0:length] * taps[0]
    result = result + padded[1 : length + 1] * taps[1]
    return result + padded[2 : length + 2] * taps[2]


def combine(earlier, later):
    return (earlier[0] * later[0], later[0][:, None, None] * earlier[1] + later[1])


def shards(
    query_proj,
    key_proj,
    value_proj,
    gate_proj,
    log_decay,
    residual,
    out_weight,
    norm_gain,
    norm_bias,
    up_gate,
    up_value,
    conv_weight,
    conv_bias,
    down_weight,
):
    tok_rows = query_proj.shape[0]
    head_count = log_decay.shape[1]
    key_width = query_proj.shape[1] // head_count
    value_width = value_proj.shape[1] // head_count
    full_gate, full_value, full_down = turned_gather(
        (up_gate, up_value, down_weight), SP, (0, 0, 1)
    )
    positions = (lax.axis_index(SP) * tok_rows + jnp.arange(tok_rows)).astype(jnp.float32)
    query_rot = rotate(
        query_proj.astype(jnp.float32).reshape(tok_rows, head_count, key_width), positions
    ).astype(jnp.bfloat16)
    key_rot = (
        rotate(key_proj.astype(jnp.float32).reshape(tok_rows, head_count, key_width), positions)
        * key_width ** (-0.5)
    ).astype(jnp.bfloat16)
    block_count = tok_rows // BLOCK
    asking_segments = query_rot.reshape(block_count, BLOCK, head_count, key_width)
    key_blocks = key_rot.reshape(block_count, BLOCK, head_count, key_width)
    value_blocks = value_proj.reshape(block_count, BLOCK, head_count, value_width)
    log_blocks = log_decay.reshape(block_count, BLOCK, head_count)
    within, scaled_query, summand_term, block_decay = jax.vmap(block_parts)(
        asking_segments, key_blocks, value_blocks, log_blocks
    )

    def absorb(carry_state, pieces):
        return (pieces[1][:, None, None] * carry_state + pieces[0], None)

    zero_state = jnp.zeros((head_count, key_width, value_width), jnp.float32)
    own_state, _ = lax.scan(absorb, zero_state, (summand_term, block_decay))
    own_decay = jnp.prod(block_decay, axis=0)
    _, incoming = entering(
        (own_decay, own_state), SP, combine, (jnp.ones_like(own_decay), zero_state)
    )

    def advance(carry_state, pieces):
        carried = jnp.einsum(
            "thd,hde->the",
            pieces[0],
            carry_state.astype(jnp.bfloat16),
            preferred_element_type=jnp.float32,
        )
        return (pieces[2][:, None, None] * carry_state + pieces[1], carried)

    _, carried = lax.scan(advance, incoming, (scaled_query, summand_term, block_decay))
    mixed_heads = (within + carried).reshape(tok_rows, head_count, value_width)
    average = mixed_heads.mean(-1, keepdims=True)
    spread = jnp.square(mixed_heads - average).mean(-1, keepdims=True)
    standardized_rows = (mixed_heads - average) * lax.rsqrt(spread + tiny_stabilizer)
    gate_heads = gate_proj.astype(jnp.float32).reshape(tok_rows, head_count, value_width)
    gated_rows = (
        (jax.nn.silu(gate_heads) * standardized_rows)
        .astype(jnp.bfloat16)
        .reshape(tok_rows, head_count * value_width)
    )
    own_count = tok_rows // lax.axis_size("tp")
    partial_rows = jnp.dot(gated_rows, out_weight, preferred_element_type=jnp.float32)
    attended = lax.psum(partial_rows.astype(jnp.bfloat16), "tp").astype(jnp.float32)
    whole_rows = layer_norm(
        alpha_scale * residual.astype(jnp.float32) + attended, norm_gain[0], norm_bias[0]
    ).astype(jnp.bfloat16)
    normed_own = lax.dynamic_slice_in_dim(
        whole_rows, lax.axis_index("tp") * own_count, own_count, 0
    )
    gate_up = jnp.dot(whole_rows, full_gate, preferred_element_type=jnp.float32)
    value_up = jnp.dot(whole_rows, full_value, preferred_element_type=jnp.float32)
    gate_up = gate_up.astype(jnp.bfloat16)
    value_up = value_up.astype(jnp.bfloat16)
    gate_edge, value_edge = passed_along((gate_up[tok_rows - 2 :], value_up[tok_rows - 2 :]), SP, 1)
    gate_conv = causal_conv(gate_up, gate_edge, conv_weight[0], conv_bias[0])
    value_conv = causal_conv(value_up, value_edge, conv_weight[1], conv_bias[1])
    activated = (jax.nn.gelu(gate_conv) * value_conv).astype(jnp.bfloat16)
    partial_ffn = jnp.dot(activated, full_down, preferred_element_type=jnp.float32)
    ffn_out = lax.psum_scatter(
        partial_ffn.astype(jnp.bfloat16), "tp", scatter_dimension=0, tiled=True
    ).astype(jnp.float32)
    return layer_norm(
        alpha_scale * normed_own.astype(jnp.float32) + ffn_out, norm_gain[1], norm_bias[1]
    ).astype(jnp.bfloat16)


def solution(mesh):
    torus = Mesh(mesh.devices.reshape(4, 4, mesh.shape["tp"]), ("sp_0", "sp_1", "tp"))
    return jax.shard_map(
        shards,
        mesh=torus,
        in_specs=(
            P(SP, "tp"),
            P(SP, "tp"),
            P(SP, "tp"),
            P(SP, "tp"),
            P(SP, "tp"),
            P(SP, None),
            P("tp", None),
            P(),
            P(),
            P(SP, "tp"),
            P(SP, "tp"),
            P(None, None, "tp"),
            P(None, "tp"),
            P("tp", SP),
        ),
        out_specs=P(SP_TP, None),
        check_vma=False,
    )
```

profile of v0, /device:TPU:0, one launch (start us, length us, event | category | flops | bytes accessed | tf_op | source)
XLA Modules:
  0.0 287.6 jit_solution(7384815758810816143)
XLA Ops:
  7.4 2.4 reduce-window.6
  10.4 1.4 bitcast_convert_fusion
  11.8 3.1 %fusion.56 = (bf16[1024,1,128]{2,0,1:T(8,128)(2,1)S(1)}, bf16[1024,1,128]{2,0,1:T(8,128)(2,1)}, f32[1024,1,128]{2,0,1:T(8,128)S(1)}, f32[1024,1,128]{2,0,1:T(8,128)S(1)}) fusion(f32[1024,1,256]{2,0,1:T(8,128)S(1)} %get-tuple-element.170, f32[128]{0:T(128)S(1)} %multiply_power_fusion, f32[1024]{0:T(1024)S(1)} %add_convert_fusion.2, ...), kind=kLoop, calls=%fused_computation.87 | loop fusion | flops 1966080 | bytes 3674624 | tf_op jit(solution)/shard_map/convert.17
  14.9 0.8 copy-done.5
  15.7 2.0 convolution_bitcast_fusion.1
  17.7 9.8 %while.24 = (s32[]{:T(128)}, f32[1,256,512]{2,1,0:T(8,128)S(1)}, f32[4,1]{0,1:T(1,128)S(1)}, f32[4,1,256,512]{3,2,1,0:T(8,128)}, s32[]{:T(128)}, /*index=5*/s32[]{:T(128)}) while((s32[]{:T(128)}, f32[1,256,512]{2,1,0:T(8,128)S(1)}, f32[4,1]{0,1:T(1,128)S(1)}, f32[4,1,256,512]{3,2,1,0:T(8,128)}, s32[]{:T(128)}, ...), condition=%wide.region_4.5_spmd.clone, body=%wide.region_3.4_spmd.clone.sunk | while | flops 393219 | bytes 1572971 | solution.py:163
  18.3 1.8 bitcast_add_fusion.8
  20.8 1.8 bitcast_add_fusion.8
  23.2 1.8 bitcast_add_fusion.8
  25.7 1.8 bitcast_add_fusion.8
  29.7 1.4 dynamic-update-slice
  31.0 10.8 %all-reduce = bf16[4]{0:T(256)(128)(2,1)S(1)} all-reduce(bf16[4]{0:T(256)(128)(2,1)S(1)} %dynamic-update-slice), channel_id=1, replica_groups=mesh['sp_0'=4,'sp_1'=4,'tp'=8] {'sp_1'}, use_global_device_ids=true, to_apply=%add | all-reduce | flops 4 | bytes 16
  43.2 11.9 %all-gather.10.cloned.1.call-done = bf16[4,256,512]{2,1,0:T(8,128)(2,1)} async-done(((bf16[1,256,512]{2,1,0:T(8,128)(2,1)}), bf16[4,256,512]{2,1,0:T(8,128)(2,1)}) %all-gather.10.cloned.1.call-update) | async-done | bytes 1048592 | tf_op jit(solution)/shard_map/all_gather | solution.py:38
  55.0 4.0 %fusion.70 = bf16[1,1,256,512]{3,2,1,0:T(8,128)(2,1)} fusion(f32[]{:T(128)} %bitcast.39, f32[]{:T(128)} %bitcast.40, f32[]{:T(128)} %bitcast.41, f32[]{:T(128)} %bitcast.42, bf16[4,256,512]{2,1,0:T(8,128)(2,1)} %all-gather.10.cloned.1.call-done), kind=kLoop, calls=%fused_computation.102 | loop fusion | flops 1572864 | bytes 1310736 | tf_op jit(solution)/shard_map/convert_element_type | solution.py:38
  60.4 1.4 dynamic-update-slice.1
  61.8 10.7 %all-reduce.1 = bf16[4]{0:T(256)(128)(2,1)S(1)} all-reduce(bf16[4]{0:T(256)(128)(2,1)S(1)} %dynamic-update-slice.1), channel_id=2, replica_groups=mesh['sp_0'=4,'sp_1'=4,'tp'=8] {'sp_0'}, use_global_device_ids=true, to_apply=%add.1 | all-reduce | flops 4 | bytes 16
  78.2 1.9 fusion.61
  80.2 3.6 %all-gather.6.cloned.1.call-done = bf16[4,1,256,512]{3,2,1,0:T(8,128)(2,1)} async-done(((bf16[1,1,256,512]{3,2,1,0:T(8,128)(2,1)}), bf16[4,1,256,512]{3,2,1,0:T(8,128)(2,1)}) %all-gather.6.cloned.1.call-update) | async-done | bytes 1048592 | tf_op jit(solution)/shard_map/all_gather | solution.py:38
  83.8 3.9 %fusion.69 = f32[1,256,512]{2,1,0:T(8,128)S(1)} fusion(bf16[4,1,256,512]{3,2,1,0:T(8,128)(2,1)} %all-gather.6.cloned.1.call-done, f32[]{:T(128)} %bitcast.39, f32[]{:T(128)} %bitcast.40, f32[]{:T(128)} %bitcast.41, f32[]{:T(128)} %bitcast.42, f32[]{:T(128)} %bitcast.33, f32[]{:T(128)S(6)} %convert.26, f32[]{:T(128)S(6)} %convert.27, f32[]{:T(128)} %bitcast.38, ...), kind=kLoop, calls=%fused_computation.99 | loop fusion | flops 4194304 | bytes 2621484 | tf_op jit(solution)/shard_map/add | solution.py:116
  87.7 17.8 %while.23 = (s32[]{:T(128)}, f32[1,256,512]{2,1,0:T(8,128)S(1)}, f32[4,256,1,512]{3,1,2,0:T(8,128)}, f32[4,1]{0,1:T(1,128)S(1)}, f32[4,1,256,512]{3,2,1,0:T(8,128)}, /*index=5*/bf16[4,256,1,256]{3,1,2,0:T(8,128)(2,1)}, s32[]{:T(128)}) while((s32[]{:T(128)}, f32[1,256,512]{2,1,0:T(8,128)S(1)}, f32[4,256,1,512]{3,1,2,0:T(8,128)}, ...), condition=%wide.region_6.7_spmd, body=%wide.region_5.6_spmd.sunk | while | flops 67502080 | bytes 2753641 | solution.py:178
  88.4 1.9 fusion.117
  90.3 1.9 bitcast_add_fusion.7
  92.8 1.9 fusion.117
  94.7 1.9 bitcast_add_fusion.7
  97.2 1.9 fusion.117
  99.2 1.9 bitcast_add_fusion.7
  101.7 1.9 fusion.117
  103.6 1.9 bitcast_add_fusion.7
  105.5 4.2 %fusion.101 = (f32[4,256]{1,0:T(4,128)S(1)}, f32[4,256,1,512]{3,1,0,2:T(8,128)}) fusion(f32[4,256,1,512]{3,1,2,0:T(8,128)} %get-tuple-element.60, bf16[4,256,512]{2,1,0:T(8,128)(2,1)} %bitcast.150, bf16[4,256,128]{2,1,0:T(8,128)(2,1)} %bitcast.155, bf16[4,256,128]{2,1,0:T(8,128)(2,1)S(1)} %bitcast.153, f32[4,256]{1,0:T(4,128)S(1)} %get-tuple-element.135, ...), kind=kOutput, calls=%fused_computation.158 | convolution fusion | flops 406846464 | bytes 6889472 | tf_op jit(solution)/shard_map/vmap(htm,mhe->the)/dot_general | solution.py:90
  109.8 2.1 multiply_reduce_fusion.1
  112.0 2.2 fusion.32
  114.2 4.3 %convolution_convert_fusion.1 = bf16[1024,2048]{1,0:T(8,128)(2,1)} fusion(bf16[1024,512]{1,0:T(8,128)(2,1)S(1)} %fusion.32, bf16[512,2048]{1,0:T(8,128)(2,1)S(1)} %copy-done), kind=kOutput, calls=%fused_computation.18 | convolution fusion | flops 2149580800 | bytes 7340032 | tf_op jit(solution)/shard_map/dot_general | solution.py:190
  119.5 0.8 pad_maximum_fusion
  120.8 71.2 %all-reduce.4.cloned.1.call-done = bf16[1024,2048]{1,0:T(8,128)(2,1)} async-done(((bf16[1024,2048]{1,0:T(8,128)(2,1)}), bf16[1024,2048]{1,0:T(8,128)(2,1)}) %all-reduce.4.cloned.1.call-update) | async-done | bytes 4194320 | tf_op jit(solution)/shard_map/psum | solution.py:191
  192.0 5.1 %fusion.6 = f32[1024]{0:T(1024)S(1)} fusion(bf16[1024,2048]{1,0:T(8,128)(2,1)} %all-reduce.4.cloned.1.call-done, bf16[1024,2048]{1,0:T(8,128)(2,1)} %param.23), kind=kLoop, calls=%fused_computation.15 | loop fusion | flops 10484736 | bytes 8392704 | tf_op jit(solution)/shard_map/reduce_sum | solution.py:74
  197.1 0.9 copy-done.2
  197.9 2.4 multiply_reduce_fusion
  200.4 4.0 %add_convert_fusion = bf16[1024,2048]{1,0:T(8,128)(2,1)} fusion(bf16[1024,2048]{1,0:T(8,128)(2,1)S(1)} %copy-done.2, bf16[1024,2048]{1,0:T(8,128)(2,1)S(1)} %copy-done.1, f32[2048]{0:T(1024)S(1)} %bitcast.164, f32[2048]{0:T(1024)S(1)} %bitcast.163, f32[1024]{0:T(1024)S(1)} %add_rsqrt_fusion, f32[1024]{0:T(1024)S(1)} %broadcast_multiply_fusion), kind=kLoop, calls=%fused_computation.12 | loop fusion | flops 18874368 | bytes 12607488 | tf_op jit(solution)/shard_map/convert_element_type | solution.py:194
  204.4 6.4 %fusion.33 = bf16[1024,704]{0,1:T(8,128)(2,1)S(1)} fusion(bf16[1024,2048]{1,0:T(8,128)(2,1)} %add_convert_fusion, bf16[2048,2112]{0,1:T(8,128)(2,1)} %all-gather.8.cloned.1.call-done), kind=kOutput, calls=%fused_computation.56 | convolution fusion | flops 2953510912 | bytes 8519680 | tf_op jit(solution)/shard_map/dot_general | solution.py:198
  210.9 3.3 %collective-permute-start = (bf16[2,704]{0,1:T(8,128)(2,1)S(1)}, bf16[2,704]{0,1:T(8,128)(2,1)S(1)}, u32[]{:S(2)}, u32[]{:S(2)}) collective-permute-start(bf16[2,704]{0,1:T(8,128)(2,1)S(1)} %slice.226), channel_id=1, source_target_pairs={{0,8},{8,16},{16,24},{24,32},{32,40},{40,48},{48,56},{56,64},{64,7... | collective-permute-start | bytes 8456 | tf_op jit(solution)/shard_map/ppermute | solution.py:56
  214.3 5.0 %fusion.36 = bf16[1024,704]{0,1:T(8,128)(2,1)S(1)} fusion(bf16[1024,2048]{1,0:T(8,128)(2,1)S(1)} %copy-done.4, bf16[2048,2112]{0,1:T(8,128)(2,1)} %all-gather.8.cloned.1.call-done), kind=kOutput, calls=%fused_computation.57 | convolution fusion | flops 2953510912 | bytes 8519680 | tf_op jit(solution)/shard_map/dot_general | solution.py:199
  219.4 3.6 %collective-permute-start.1 = (bf16[2,704]{0,1:T(8,128)(2,1)S(1)}, bf16[2,704]{0,1:T(8,128)(2,1)S(1)}, u32[]{:S(2)}, u32[]{:S(2)}) collective-permute-start(bf16[2,704]{0,1:T(8,128)(2,1)S(1)} %slice.231), channel_id=1, source_target_pairs={{0,8},{8,16},{16,24},{24,32},{32,40},{40,48},{48,56},{56,64},{64,7... | collective-permute-start | bytes 8456 | tf_op jit(solution)/shard_map/ppermute | solution.py:56
  223.8 2.0 collective-permute-done.1
  226.6 10.0 %convolution_convert_fusion = bf16[1024,2048]{1,0:T(8,128)(2,1)} fusion(bf16[2048,2112]{0,1:T(8,128)(2,1)} %all-gather.8.cloned.1.call-done, f32[1026,704]{0,1:T(8,128)S(1)} %maximum_convert_fusion.1, f32[1026,704]{0,1:T(8,128)S(1)} %maximum_convert_fusion, f32[704]{0:T(1024)S(1)} %get-tuple-element.110, f32[704]{0:T(1024)S(1)} %get-tuple-element.111, ...), kind=kOutput, calls=%fused_computation.17 | convolution fusion | flops 2970746880 | bytes 24412160 | tf_op jit(solution)/shard_map/dot_general | solution.py:206
  236.6 38.6 %reduce-scatter.2.cloned.1.call-done = bf16[128,2048]{1,0:T(8,128)(2,1)} async-done(((bf16[1024,2048]{1,0:T(8,128)(2,1)}), bf16[128,2048]{1,0:T(8,128)(2,1)}) %reduce-scatter.2.cloned.1.call-update) | async-done | bytes 524304 | tf_op jit(solution)/shard_map/reduce_scatter | solution.py:207
  275.2 1.5 fusion.46
  276.7 1.5 multiply_reduce_fusion.2
  278.2 2.3 add_convert_fusion.1
  (90 shorter events, 13.6 us)
Async XLA Ops:
  7.4 106.8 %copy-start = (bf16[512,2048]{1,0:T(8,128)(2,1)S(1)}, bf16[512,2048]{1,0:T(8,128)(2,1)}, u32[]{:S(2)}) copy-start(bf16[512,2048]{1,0:T(8,128)(2,1)} %param.24) | copy-start | bytes 6291460
  7.4 47.7 %all-gather.10.cloned.1.call-start = ((), (), s32[]{:S(2)}) async-start(), calls=%async_computation.5 | async-start | bytes 1310720 | tf_op jit(solution)/shard_map/all_gather | solution.py:38
  10.4 5.3 %copy-start.6 = (bf16[1024,512]{1,0:T(8,128)(2,1)S(1)}, bf16[1024,512]{1,0:T(8,128)(2,1)}, u32[]{:S(2)}) copy-start(bf16[1024,512]{1,0:T(8,128)(2,1)} %param.20) | copy-start | bytes 3145732
  14.9 0.8 copy-start.5
  17.7 10.6 %copy-start.15 = (u32[128]{0:T(128)S(1)}, u32[128]{0:T(128)}, u32[]{:S(2)}) copy-start(u32[128]{0:T(128)} %constant.102) | copy-start | bytes 1540
  17.7 41.3 %copy-start.14 = (u32[128]{0:T(128)S(1)}, u32[128]{0:T(128)}, u32[]{:S(2)}) copy-start(u32[128]{0:T(128)} %constant.107) | copy-start | bytes 1540
  28.3 55.6 %all-gather.6.cloned.1.call-start = ((), (), s32[]{:S(2)}) async-start(), calls=%async_computation.1 | async-start | bytes 1310720 | tf_op jit(solution)/shard_map/all_gather | solution.py:38
  59.0 133.0 %all-reduce.4.cloned.1.call-start = ((), (), s32[]{:S(2)}) async-start(), calls=%async_computation.2 | async-start | bytes 8388608 | tf_op jit(solution)/shard_map/psum | solution.py:191
  109.7 2.2 copy-start.3
  118.4 0.9 copy-start.7
  118.5 1.0 copy-start.8
  118.5 1.1 copy-start.9
  118.5 2.2 copy-start.13
  118.5 2.2 copy-start.10
  118.5 2.3 copy-start.11
  118.5 2.3 copy-start.12
  118.5 85.9 %all-gather.8.cloned.1.call-start = ((), (), s32[]{:S(2)}) async-start(), calls=%async_computation.3 | async-start | bytes 9191424 | tf_op jit(solution)/shard_map/all_gather | solution.py:18
  120.4 154.8 %reduce-scatter.2.cloned.1.call-start = ((), (), s32[]{:S(2)}) async-start(), calls=%async_computation.4 | async-start | bytes 4718592 | tf_op jit(solution)/shard_map/reduce_scatter | solution.py:207
  192.0 5.1 %copy-start.1 = (bf16[1024,2048]{1,0:T(8,128)(2,1)S(1)}, bf16[1024,2048]{1,0:T(8,128)(2,1)}, u32[]{:S(2)}) copy-start(bf16[1024,2048]{1,0:T(8,128)(2,1)} %param.23) | copy-start | bytes 12582916
  192.0 6.0 %copy-start.2 = (bf16[1024,2048]{1,0:T(8,128)(2,1)S(1)}, bf16[1024,2048]{1,0:T(8,128)(2,1)}, u32[]{:S(2)}) copy-start(bf16[1024,2048]{1,0:T(8,128)(2,1)} %all-reduce.4.cloned.1.call-done) | copy-start | bytes 12582916
  204.4 9.9 %copy-start.4 = (bf16[1024,2048]{1,0:T(8,128)(2,1)S(1)}, bf16[1024,2048]{1,0:T(8,128)(2,1)}, u32[]{:S(2)}) copy-start(bf16[1024,2048]{1,0:T(8,128)(2,1)} %add_convert_fusion) | copy-start | bytes 12582916
  210.9 12.1 %collective-permute-start = (bf16[2,704]{0,1:T(8,128)(2,1)S(1)}, bf16[2,704]{0,1:T(8,128)(2,1)S(1)}, u32[]{:S(2)}, u32[]{:S(2)}) collective-permute-start(bf16[2,704]{0,1:T(8,128)(2,1)S(1)} %slice.226), channel_id=1, source_target_pairs={{0,8},{8,16},{16,24},{24,32},{32,40},{40,48},{48,56},{56,64},{64,7... | collective-permute-start | bytes 8456 | tf_op jit(solution)/shard_map/ppermute | solution.py:56
  219.4 6.4 %collective-permute-start.1 = (bf16[2,704]{0,1:T(8,128)(2,1)S(1)}, bf16[2,704]{0,1:T(8,128)(2,1)S(1)}, u32[]{:S(2)}, u32[]{:S(2)}) collective-permute-start(bf16[2,704]{0,1:T(8,128)(2,1)S(1)} %slice.231), channel_id=1, source_target_pairs={{0,8},{8,16},{16,24},{24,32},{32,40},{40,48},{48,56},{56,64},{64,7... | collective-permute-start | bytes 8456 | tf_op jit(solution)/shard_map/ppermute | solution.py:56
Sparse Core Ops, SparseCore 0:
  28.4 26.5 all-gather.9
  59.1 24.6 all-gather.5
  118.6 73.2 all-reduce.3
  236.7 38.4 reduce-scatter.1
Sparse Core Ops, SparseCore 1:
  121.1 78.5 all-gather.7
where the time goes:
time: 289 us; the launch traced here: 288 us
  waiting for transfers between devices  127 us (44%)
  other arithmetic  58 us (20%)
  matrix products  39.6 us (14%)
  blocking collectives  21.5 us (7%)
  between operations  20.6 us (7%)
  local copies, waits for them, and re-layouts  13.1 us (5%)
  starting transfers between devices  7.31 us (3%)
    psum x1, waiting for transfers between devices, shards(): lax.psum(partial_rows.astype(jnp.bfloat16), 'tp').astype(jnp.float32)  71.2 us
    reduce_scatter x1, waiting for transfers between devices, shards(): lax.psum_scatter(partial_ffn.astype(jnp.bfloat16), 'tp', scatter_dimensio...  38.6 us
    unnamed x2, blocking collectives  21.5 us
    all_gather x2, waiting for transfers between devices, entering(): lax.all_gather(part.astype(kind), axis)  15.5 us
    dot_general x1, matrix products, shards(): jnp.dot(activated, full_down, preferred_element_type=jnp.float32)  9.97 us
    dot_general x4, matrix products, advance(): jnp.einsum('thd,hde->the', pieces[0], carry_state.astype(jnp.bfloat16), p...  7.74 us
    add x4, other arithmetic, advance(): return (pieces[2][:, None, None] * carry_state + pieces[1], carried)  7.52 us
    add x4, other arithmetic, absorb(): return (pieces[1][:, None, None] * carry_state + pieces[0], None)  7.35 us
  transfers between devices with their start and end apart: 7, of which 5 were waited for; matrix products, arithmetic and copies ran while one was open for 9% of the time, Pallas kernels for 0%

commit v1 on v0

--- a/solution.py
+++ b/solution.py
@@ -188,7 +188,9 @@
     )
     own_count = tok_rows // lax.axis_size("tp")
     partial_rows = jnp.dot(gated_rows, out_weight, preferred_element_type=jnp.float32)
-    attended = lax.psum(partial_rows.astype(jnp.bfloat16), "tp").astype(jnp.float32)
+    attended = jnp.sum(lax.all_gather(partial_rows.astype(jnp.bfloat16), "tp"), axis=0).astype(
+        jnp.float32
+    )
     whole_rows = layer_norm(
         alpha_scale * residual.astype(jnp.float32) + attended, norm_gain[0], norm_bias[0]
     ).astype(jnp.bfloat16)

time: 289 us -> 440 us (1.52)
  waiting for transfers between devices: 127 us -> 267 us
  other arithmetic: 58 us -> 72.1 us
    all_gather x0 -> x1, waiting for transfers between devices: none -> 154 us  [shards(): lax.all_gather(partial_rows.astype(jnp.bfloat16), 'tp')]
    psum x1 -> x0, waiting for transfers between devices: 71.2 us -> none  [shards(): lax.psum(partial_rows.astype(jnp.bfloat16), 'tp').astype(jnp.float32)]
    all_gather x1, waiting for transfers between devices: 0.01 us -> 55.1 us  [turned_gather(): out, at, finished = (lax.all_gather(both, axis, axis=0, tiled=True), 0, [])]
    reduce_sum x0 -> x1, other arithmetic: none -> 14.1 us  [shards(): jnp.sum(lax.all_gather(partial_rows.astype(jnp.bfloat16), 'tp'), axis=0)]
  transfers between devices with their start and end apart: 7 -> 7, of which waited for: 5 -> 6; matrix products, arithmetic and copies ran while one was open for 9% -> 9% of each run, Pallas kernels for 0% -> 0%
where the time goes in v1:
time: 440 us; the launch traced here: 439 us
  waiting for transfers between devices  267 us (61%)
  other arithmetic  72.1 us (16%)
  matrix products  39.7 us (9%)
  blocking collectives  21.5 us (5%)
  between operations  19.2 us (4%)
  local copies, waits for them, and re-layouts  13.1 us (3%)
  starting transfers between devices  5.82 us (1%)
    all_gather x1, waiting for transfers between devices, shards(): lax.all_gather(partial_rows.astype(jnp.bfloat16), 'tp')  154 us
    all_gather x1, waiting for transfers between devices, turned_gather(): out, at, finished = (lax.all_gather(both, axis, axis=0, tiled=True), 0, [])  55.1 us
    reduce_scatter x1, waiting for transfers between devices, shards(): lax.psum_scatter(partial_ffn.astype(jnp.bfloat16), 'tp', scatter_dimensio...  40.8 us
    unnamed x2, blocking collectives  21.5 us
    all_gather x2, waiting for transfers between devices, entering(): lax.all_gather(part.astype(kind), axis)  15.5 us
    reduce_sum x1, other arithmetic, shards(): jnp.sum(lax.all_gather(partial_rows.astype(jnp.bfloat16), 'tp'), axis=0)  14.1 us
    dot_general x1, matrix products, shards(): jnp.dot(activated, full_down, preferred_element_type=jnp.float32)  10 us
  transfers between devices with their start and end apart: 7, of which 6 were waited for; matrix products, arithmetic and copies ran while one was open for 9% of the time, Pallas kernels for 0%

profile of v1, /device:TPU:0, one launch (start us, length us, event | category | flops | bytes accessed | tf_op | source)
XLA Modules:
  0.0 438.9 jit_solution(2436347418698351199)
XLA Ops:
  6.6 2.4 reduce-window.6
  9.4 1.4 bitcast_convert_fusion
  11.0 3.0 fusion.56
  14.8 2.0 convolution_bitcast_fusion.1
  16.9 9.8 %while.24 = (s32[]{:T(128)}, f32[1,256,512]{2,1,0:T(8,128)S(1)}, f32[4,1]{0,1:T(1,128)S(1)}, f32[4,1,256,512]{3,2,1,0:T(8,128)}, s32[]{:T(128)}, /*index=5*/s32[]{:T(128)}) while((s32[]{:T(128)}, f32[1,256,512]{2,1,0:T(8,128)S(1)}, f32[4,1]{0,1:T(1,128)S(1)}, f32[4,1,256,512]{3,2,1,0:T(8,128)}, s32[]{:T(128)}, ...), condition=%wide.region_4.5_spmd.clone, body=%wide.region_3.4_spmd.clone.sunk | while | flops 393219 | bytes 1572963 | solution.py:163
  17.5 1.8 bitcast_add_fusion.8
  19.9 1.8 bitcast_add_fusion.8
  22.3 1.8 bitcast_add_fusion.8
  24.8 1.8 bitcast_add_fusion.8
  28.8 1.4 dynamic-update-slice
  30.2 10.8 %all-reduce = bf16[4]{0:T(256)(128)(2,1)S(1)} all-reduce(bf16[4]{0:T(256)(128)(2,1)S(1)} %dynamic-update-slice), channel_id=1, replica_groups=mesh['sp_0'=4,'sp_1'=4,'tp'=8] {'sp_1'}, use_global_device_ids=true, to_apply=%add | all-reduce | flops 4 | bytes 16
  42.3 11.9 %all-gather.12.cloned.1.call-done = bf16[4,256,512]{2,1,0:T(8,128)(2,1)} async-done(((bf16[1,256,512]{2,1,0:T(8,128)(2,1)}), bf16[4,256,512]{2,1,0:T(8,128)(2,1)}) %all-gather.12.cloned.1.call-update) | async-done | bytes 1048592 | tf_op jit(solution)/shard_map/all_gather | solution.py:38
  54.2 4.0 fusion.70
  59.5 1.4 dynamic-update-slice.1
  60.9 10.7 %all-reduce.1 = bf16[4]{0:T(256)(128)(2,1)S(1)} all-reduce(bf16[4]{0:T(256)(128)(2,1)S(1)} %dynamic-update-slice.1), channel_id=2, replica_groups=mesh['sp_0'=4,'sp_1'=4,'tp'=8] {'sp_0'}, use_global_device_ids=true, to_apply=%add.1 | all-reduce | flops 4 | bytes 16
  77.3 1.9 fusion.61
  79.3 3.7 all-gather.8.cloned.1.call-done
  83.0 3.9 fusion.69
  86.9 17.8 %while.23 = (s32[]{:T(128)}, f32[1,256,512]{2,1,0:T(8,128)S(1)}, f32[4,256,1,512]{3,1,2,0:T(8,128)}, f32[4,1]{0,1:T(1,128)S(1)}, f32[4,1,256,512]{3,2,1,0:T(8,128)}, /*index=5*/bf16[4,256,1,256]{3,1,2,0:T(8,128)(2,1)}, s32[]{:T(128)}) while((s32[]{:T(128)}, f32[1,256,512]{2,1,0:T(8,128)S(1)}, f32[4,256,1,512]{3,1,2,0:T(8,128)}, ...), condition=%wide.region_6.7_spmd, body=%wide.region_5.6_spmd.sunk | while | flops 67502080 | bytes 2753633 | solution.py:178
  86.9 1.9 fusion.117
  89.5 1.9 bitcast_add_fusion.7
  91.4 1.9 fusion.117
  93.9 1.9 bitcast_add_fusion.7
  95.8 1.9 fusion.117
  98.3 1.9 bitcast_add_fusion.7
  100.2 1.9 fusion.117
  102.8 1.9 bitcast_add_fusion.7
  104.7 4.2 fusion.101
  108.9 2.1 multiply_reduce_fusion.1
  111.1 2.2 fusion.32
  113.3 4.3 convolution_convert_fusion.1
  120.0 153.9 %all-gather.14.cloned.1.call-done = bf16[8192,2048]{1,0:T(8,128)(2,1)} async-done(((bf16[1024,2048]{1,0:T(8,128)(2,1)}), bf16[8192,2048]{1,0:T(8,128)(2,1)}) %all-gather.14.cloned.1.call-update) | async-done | bytes 33554448 | tf_op jit(solution)/shard_map/all_gather | solution.py:191
  273.9 14.1 %reduce_sum.68 = bf16[1024,2048]{1,0:T(8,128)(2,1)} reduce(bf16[8,1024,2048]{2,1,0:T(8,128)(2,1)} %bitcast.147, bf16[]{:T(256)} %constant.93.clone.1), dimensions={0}, to_apply=%region_9.10 | reduce | flops 14680064 | bytes 37748736 | tf_op jit(solution)/shard_map/reduce_sum | solution.py:191
  288.0 5.1 %fusion.6 = f32[1024]{0:T(1024)S(1)} fusion(bf16[1024,2048]{1,0:T(8,128)(2,1)} %reduce_sum.68, bf16[1024,2048]{1,0:T(8,128)(2,1)} %param.23), kind=kLoop, calls=%fused_computation.15 | loop fusion | flops 10484736 | bytes 8392704 | tf_op jit(solution)/shard_map/reduce_sum | solution.py:74
  293.1 0.9 copy-done.3
  294.0 2.4 multiply_reduce_fusion
  296.4 4.0 add_convert_fusion
  300.4 55.1 %all-gather.10.cloned.1.call-done = bf16[2048,2112]{0,1:T(8,128)(2,1)} async-done(((bf16[128,2112]{0,1:T(8,128)(2,1)}), bf16[2048,2112]{0,1:T(8,128)(2,1)}) %all-gather.10.cloned.1.call-update) | async-done | bytes 8650768 | tf_op jit(solution)/shard_map/all_gather | solution.py:18
  355.5 6.4 %fusion.33 = bf16[1024,704]{0,1:T(8,128)(2,1)S(1)} fusion(bf16[1024,2048]{1,0:T(8,128)(2,1)} %add_convert_fusion, bf16[2048,2112]{0,1:T(8,128)(2,1)} %all-gather.10.cloned.1.call-done), kind=kOutput, calls=%fused_computation.56 | convolution fusion | flops 2953510912 | bytes 8519680 | tf_op jit(solution)/shard_map/dot_general | solution.py:200
  362.1 3.1 collective-permute-start
  365.2 5.0 %fusion.36 = bf16[1024,704]{0,1:T(8,128)(2,1)S(1)} fusion(bf16[1024,2048]{1,0:T(8,128)(2,1)S(1)} %copy-done.5, bf16[2048,2112]{0,1:T(8,128)(2,1)} %all-gather.10.cloned.1.call-done), kind=kOutput, calls=%fused_computation.57 | convolution fusion | flops 2953510912 | bytes 8519680 | tf_op jit(solution)/shard_map/dot_general | solution.py:201
  370.3 2.4 collective-permute-start.1
  373.5 2.0 collective-permute-done.1
  376.2 10.0 %convolution_convert_fusion = bf16[1024,2048]{1,0:T(8,128)(2,1)} fusion(bf16[2048,2112]{0,1:T(8,128)(2,1)} %all-gather.10.cloned.1.call-done, f32[1026,704]{0,1:T(8,128)S(1)} %maximum_convert_fusion.1, f32[1026,704]{0,1:T(8,128)S(1)} %maximum_convert_fusion, f32[704]{0:T(1024)S(1)} %get-tuple-element.110, f32[704]{0:T(1024)S(1)} %get-tuple-element.111, ...), kind=kOutput, calls=%fused_computation.17 | convolution fusion | flops 2970746880 | bytes 24412160 | tf_op jit(solution)/shard_map/dot_general | solution.py:208
  386.3 40.8 %reduce-scatter.2.cloned.1.call-done = bf16[128,2048]{1,0:T(8,128)(2,1)} async-done(((bf16[1024,2048]{1,0:T(8,128)(2,1)}), bf16[128,2048]{1,0:T(8,128)(2,1)}) %reduce-scatter.2.cloned.1.call-update) | async-done | bytes 524304 | tf_op jit(solution)/shard_map/reduce_scatter | solution.py:209
  427.1 1.5 fusion.46
  428.5 1.5 multiply_reduce_fusion.2
  430.1 2.3 add_convert_fusion.1
  (93 shorter events, 15.2 us)
Async XLA Ops:
  6.5 106.8 %copy-start = (bf16[512,2048]{1,0:T(8,128)(2,1)S(1)}, bf16[512,2048]{1,0:T(8,128)(2,1)}, u32[]{:S(2)}) copy-start(bf16[512,2048]{1,0:T(8,128)(2,1)} %param.24) | copy-start | bytes 6291460
  6.5 47.6 %all-gather.12.cloned.1.call-start = ((), (), s32[]{:S(2)}) async-start(), calls=%async_computation.4 | async-start | bytes 1310720 | tf_op jit(solution)/shard_map/all_gather | solution.py:38
  9.4 5.4 %copy-start.7 = (bf16[1024,512]{1,0:T(8,128)(2,1)S(1)}, bf16[1024,512]{1,0:T(8,128)(2,1)}, u32[]{:S(2)}) copy-start(bf16[1024,512]{1,0:T(8,128)(2,1)} %param.20) | copy-start | bytes 3145732
  14.0 0.8 copy-start.6
  16.9 10.6 %copy-start.16 = (u32[128]{0:T(128)S(1)}, u32[128]{0:T(128)}, u32[]{:S(2)}) copy-start(u32[128]{0:T(128)} %constant.104) | copy-start | bytes 1540
  16.9 41.4 %copy-start.15 = (u32[128]{0:T(128)S(1)}, u32[128]{0:T(128)}, u32[]{:S(2)}) copy-start(u32[128]{0:T(128)} %constant.109) | copy-start | bytes 1540
  27.4 55.6 %all-gather.8.cloned.1.call-start = ((), (), s32[]{:S(2)}) async-start(), calls=%async_computation.1 | async-start | bytes 1310720 | tf_op jit(solution)/shard_map/all_gather | solution.py:38
  58.2 215.7 %all-gather.14.cloned.1.call-start = ((), (), s32[]{:S(2)}) async-start(), calls=%async_computation.5 | async-start | bytes 37748736 | tf_op jit(solution)/shard_map/all_gather | solution.py:191
  108.9 2.2 copy-start.4
  117.6 0.9 copy-start.8
  117.6 1.0 copy-start.9
  117.6 1.1 copy-start.10
  117.6 2.2 copy-start.14
  117.6 2.2 copy-start.11
  117.6 2.3 copy-start.12
  117.7 2.3 copy-start.13
  117.7 237.8 %all-gather.10.cloned.1.call-start = ((), (), s32[]{:S(2)}) async-start(), calls=%async_computation.2 | async-start | bytes 9191424 | tf_op jit(solution)/shard_map/all_gather | solution.py:18
  119.6 307.5 %reduce-scatter.2.cloned.1.call-start = ((), (), s32[]{:S(2)}) async-start(), calls=%async_computation.3 | async-start | bytes 4718592 | tf_op jit(solution)/shard_map/reduce_scatter | solution.py:209
  288.0 5.1 %copy-start.2 = (bf16[1024,2048]{1,0:T(8,128)(2,1)S(1)}, bf16[1024,2048]{1,0:T(8,128)(2,1)}, u32[]{:S(2)}) copy-start(bf16[1024,2048]{1,0:T(8,128)(2,1)} %reduce_sum.68) | copy-start | bytes 12582916
  288.0 6.0 %copy-start.3 = (bf16[1024,2048]{1,0:T(8,128)(2,1)S(1)}, bf16[1024,2048]{1,0:T(8,128)(2,1)}, u32[]{:S(2)}) copy-start(bf16[1024,2048]{1,0:T(8,128)(2,1)} %param.23) | copy-start | bytes 12582916
  355.5 9.7 %copy-start.5 = (bf16[1024,2048]{1,0:T(8,128)(2,1)S(1)}, bf16[1024,2048]{1,0:T(8,128)(2,1)}, u32[]{:S(2)}) copy-start(bf16[1024,2048]{1,0:T(8,128)(2,1)} %add_convert_fusion) | copy-start | bytes 12582916
  362.1 10.6 %collective-permute-start = (bf16[2,704]{0,1:T(8,128)(2,1)S(1)}, bf16[2,704]{0,1:T(8,128)(2,1)S(1)}, u32[]{:S(2)}, u32[]{:S(2)}) collective-permute-start(bf16[2,704]{0,1:T(8,128)(2,1)S(1)} %slice.226), channel_id=1, source_target_pairs={{0,8},{8,16},{16,24},{24,32},{32,40},{40,48},{48,56},{56,64},{64,7... | collective-permute-start | bytes 8456 | tf_op jit(solution)/shard_map/ppermute | solution.py:56
  370.3 5.1 %collective-permute-start.1 = (bf16[2,704]{0,1:T(8,128)(2,1)S(1)}, bf16[2,704]{0,1:T(8,128)(2,1)S(1)}, u32[]{:S(2)}, u32[]{:S(2)}) collective-permute-start(bf16[2,704]{0,1:T(8,128)(2,1)S(1)} %slice.231), channel_id=1, source_target_pairs={{0,8},{8,16},{16,24},{24,32},{32,40},{40,48},{48,56},{56,64},{64,7... | collective-permute-start | bytes 8456 | tf_op jit(solution)/shard_map/ppermute | solution.py:56
  386.3 46.1 %copy-start.1 = (bf16[512,2048]{1,0:T(8,128)(2,1)S(1)}, bf16[512,2048]{1,0:T(8,128)(2,1)}, u32[]{:S(2)}) copy-start(bf16[512,2048]{1,0:T(8,128)(2,1)} %param.24) | copy-start | bytes 6291460
Sparse Core Ops, SparseCore 0:
  27.5 26.5 all-gather.11
  58.3 24.6 all-gather.7
  117.8 156.0 all-gather.13
  275.9 79.6 all-gather.9
  386.4 40.6 reduce-scatter.1
